TPU v7x, 32 devices: a whole 2x2x4 slice. The times are simulated.
32 devices in a mesh: rep: 4 (over z), fs: 4 (over y, x), tp: 2 (over core).
Axes of the slice: x: 2, y: 2, z: 4, core: 2. Of those that a mesh axis runs over, the one named last changes fastest.
Arguments:
- tokens: bfloat16 [16, 768, 2048], P(('rep', 'fs')), may hold values from -6 to 6
- norm_gain: float32 [2048], replicated, may hold values from 0.1 to 1.9
- outer_weight: bfloat16 [2048, 2048], P('fs', 'tp'), may hold values from -0.125 to 0.125
- inner_weight: bfloat16 [2048, 2048], P('fs', 'tp'), may hold values from -0.125 to 0.125
- value_weight: bfloat16 [2048, 2048], P('fs', 'tp'), may hold values from -0.125 to 0.125
- conv_taps: float32 [3, 2048], replicated, may hold values from -3.5 to 3.5
- out_weight: bfloat16 [2048, 2048], P('fs', 'tp'), may hold values from -0.125 to 0.125
Outputs:
- mixed: bfloat16 [16, 768, 2048], P(('rep', 'fs'), None, 'tp')
All inputs are finite; a program needn't handle non-finite values.
Results may differ from a plain program's by a relative error of at most 0.014.
Values may be sent and summed in bfloat16 or wider, within the bound.
A program may use at most 64 MiB of HBM per device.

v0:
```python
import jax
import jax.numpy as jnp
from jax import lax
from jax.sharding import PartitionSpec as P


def local(tokens, norm_gain, outer_weight, inner_weight, value_weight, conv_taps, out_weight):
    seq_len = tokens.shape[1]
    width = tokens.shape[2]
    xf = tokens.reshape(seq_len, width).astype(jnp.float32)
    scale = lax.rsqrt(jnp.mean(xf * xf, axis=-1, keepdims=True) + 1e-06)
    normed = (xf * scale * norm_gain).astype(jnp.bfloat16)
    columns = outer_weight.shape[1]

    def add_piece(piece):
        return jnp.dot(normed, piece, preferred_element_type=jnp.float32)

    outer = add_piece(lax.all_gather(outer_weight, "fs", axis=0, tiled=True))
    inner = add_piece(lax.all_gather(inner_weight, "fs", axis=0, tiled=True))
    value = add_piece(lax.all_gather(value_weight, "fs", axis=0, tiled=True))
    outer = outer.astype(jnp.bfloat16)
    inner = inner.astype(jnp.bfloat16)
    value = value.astype(jnp.bfloat16)
    product = inner.astype(jnp.float32) * value.astype(jnp.float32)
    offset = lax.axis_index("tp") * columns
    taps = lax.dynamic_slice_in_dim(conv_taps, offset, columns, 1)
    count = conv_taps.shape[0]
    padded = jnp.pad(product, ((count - 1, 0), (0, 0)))
    convolved = jnp.zeros((seq_len, columns), jnp.float32)
    for k in range(count):
        convolved = convolved + taps[k] * padded[k : k + seq_len, :]
    gated = (outer.astype(jnp.float32) * convolved).astype(jnp.bfloat16)
    everything = lax.all_gather(gated, "tp", axis=1, tiled=True)
    result = jnp.dot(
        everything,
        lax.all_gather(out_weight, "fs", axis=0, tiled=True),
        preferred_element_type=jnp.float32,
    )
    return result.astype(jnp.bfloat16).reshape(1, seq_len, columns)


def solution(mesh):
    in_specs = (
        P(("rep", "fs"), None, None),
        P(),
        P("fs", "tp"),
        P("fs", "tp"),
        P("fs", "tp"),
        P(),
        P("fs", "tp"),
    )
    out_specs = P(("rep", "fs"), None, "tp")
    return jax.shard_map(local, mesh=mesh, in_specs=in_specs, out_specs=out_specs, check_vma=False)
```

profile of v0, /device:TPU:0, one launch (start us, length us, event | category | flops | bytes accessed | tf_op | source)
XLA Modules:
  0.0 255.5 jit_solution(18304229545955920664)
XLA Ops:
  6.5 0.0 copy-start
  6.5 0.0 all-gather.8.cloned.1.call-start
  6.5 0.7 all-gather.8.cloned.1.call-update
  7.3 0.0 copy-start.1
  7.3 0.0 all-gather.10.cloned.1.call-start
  7.3 0.7 all-gather.10.cloned.1.call-update
  8.0 0.0 all-gather.6.cloned.1.call-start
  8.1 0.7 all-gather.6.cloned.1.call-update
  8.8 0.0 all-gather.14.cloned.1.call-start
  8.8 0.5 all-gather.14.cloned.1.call-update
  9.3 0.0 all-gather.12.cloned.1.call-start
  9.4 0.9 constant_dynamic-slice_fusion
  10.3 0.0 copy-done
  10.3 0.7 fusion
  11.0 53.5 %all-gather.8.cloned.1.call-done = bf16[2048,1024]{1,0:T(8,128)(2,1)} async-done(((bf16[512,1024]{1,0:T(8,128)(2,1)}), bf16[2048,1024]{1,0:T(8,128)(2,1)}) %all-gather.8.cloned.1.call-update) | async-done | bytes 4194320 | tf_op jit(solution)/shard_map/all_gather | solution.py:19
  64.5 0.0 copy-done.1
  64.5 6.8 %convolution_convert_fusion.2 = bf16[768,1024]{1,0:T(8,128)(2,1)} fusion(bf16[2048,1024]{1,0:T(8,128)(2,1)} %all-gather.8.cloned.1.call-done, bf16[1,768,2048]{2,1,0:T(8,128)(2,1)S(1)} %copy-done, f32[2048]{0:T(1024)S(1)} %copy-done.1, f32[768]{0:T(1024)S(1)} %add_rsqrt_fusion), kind=kOutput, calls=%fused_computation.9 | convolution fusion | flops 3228303360 | bytes 8924160 | tf_op jit(solution)/shard_map/dot_general | solution.py:16
  71.3 47.6 %all-gather.10.cloned.1.call-done = bf16[2048,1024]{1,0:T(8,128)(2,1)} async-done(((bf16[512,1024]{1,0:T(8,128)(2,1)}), bf16[2048,1024]{1,0:T(8,128)(2,1)}) %all-gather.10.cloned.1.call-update) | async-done | bytes 4194320 | tf_op jit(solution)/shard_map/all_gather | solution.py:20
  119.0 7.4 %convert_multiply_fusion.2 = f32[768,1024]{1,0:T(8,128)} fusion(bf16[768,1024]{1,0:T(8,128)(2,1)} %convolution_convert_fusion.2, bf16[2048,1024]{1,0:T(8,128)(2,1)} %all-gather.10.cloned.1.call-done, bf16[1,768,2048]{2,1,0:T(8,128)(2,1)S(1)} %copy-done, f32[2048]{0:T(1024)S(1)} %copy-done.1, f32[768]{0:T(1024)S(1)} %add_rsqrt_fusion), kind=kOutput, calls=%fused_computation.6 | convolution fusion | flops 3230662656 | bytes 12069888 | tf_op jit(solution)/shard_map/dot_general | solution.py:16
  126.3 47.1 %all-gather.6.cloned.1.call-done = bf16[2048,1024]{1,0:T(8,128)(2,1)} async-done(((bf16[512,1024]{1,0:T(8,128)(2,1)}), bf16[2048,1024]{1,0:T(8,128)(2,1)}) %all-gather.6.cloned.1.call-update) | async-done | bytes 4194320 | tf_op jit(solution)/shard_map/all_gather | solution.py:18
  173.4 9.4 %multiply_convert_fusion = bf16[768,1024]{1,0:T(8,128)(2,1)} fusion(f32[768,1024]{1,0:T(8,128)} %convert_multiply_fusion.2, f32[1024]{0:T(1024)S(1)} %bitcast.19, f32[1024]{0:T(1024)S(1)} %bitcast.18, f32[1024]{0:T(1024)S(1)} %bitcast.17, bf16[2048,1024]{1,0:T(8,128)(2,1)} %all-gather.6.cloned.1.call-done, bf16[1,768,2048]{2,1,0:T(8,128)(2,1)S(1)} %copy-done, ...), kind=kOutput, calls=%fused_computation.5 | convolution fusion | flops 3234594816 | bytes 12082176 | tf_op jit(solution)/shard_map/dot_general | solution.py:16
  182.8 0.0 all-gather.12.cloned.1.call-update
  182.8 44.9 %all-gather.14.cloned.1.call-done = bf16[2048,1024]{1,0:T(8,128)(2,1)} async-done(((bf16[512,1024]{1,0:T(8,128)(2,1)}), bf16[2048,1024]{1,0:T(8,128)(2,1)}) %all-gather.14.cloned.1.call-update) | async-done | bytes 4194320 | tf_op jit(solution)/shard_map/all_gather | solution.py:36
  227.7 13.5 %all-gather.12.cloned.1.call-done = bf16[768,2048]{1,0:T(8,128)(2,1)} async-done(((bf16[768,1024]{1,0:T(8,128)(2,1)}), bf16[768,2048]{1,0:T(8,128)(2,1)}) %all-gather.12.cloned.1.call-update) | async-done | bytes 3145744 | tf_op jit(solution)/shard_map/all_gather | solution.py:33
  241.2 7.7 %fusion.3 = bf16[1,768,1024]{2,1,0:T(8,128)(2,1)} fusion(bf16[768,2048]{1,0:T(8,128)(2,1)} %all-gather.12.cloned.1.call-done, bf16[2048,1024]{1,0:T(8,128)(2,1)} %all-gather.14.cloned.1.call-done), kind=kOutput, calls=%fused_computation.11 | convolution fusion | flops 3222011904 | bytes 8912896 | tf_op jit(solution)/shard_map/dot_general | solution.py:34
  (1 shorter events, 0.0 us)
Async XLA Ops:
  6.5 3.8 %copy-start = (bf16[1,768,2048]{2,1,0:T(8,128)(2,1)S(1)}, bf16[1,768,2048]{2,1,0:T(8,128)(2,1)}, u32[]{:S(2)}) copy-start(bf16[1,768,2048]{2,1,0:T(8,128)(2,1)} %param.7) | copy-start | bytes 9437188
  6.5 58.0 %all-gather.8.cloned.1.call-start = ((), (), s32[]{:S(2)}) async-start(), calls=%async_computation.1 | async-start | bytes 5242880 | tf_op jit(solution)/shard_map/all_gather | solution.py:19
  7.3 57.3 %copy-start.1 = (f32[2048]{0:T(1024)S(1)}, f32[2048]{0:T(1024)}, u32[]{:S(2)}) copy-start(f32[2048]{0:T(1024)} %param.8) | copy-start | bytes 24580
  7.3 111.7 %all-gather.10.cloned.1.call-start = ((), (), s32[]{:S(2)}) async-start(), calls=%async_computation.2 | async-start | bytes 5242880 | tf_op jit(solution)/shard_map/all_gather | solution.py:20
  8.0 165.4 %all-gather.6.cloned.1.call-start = ((), (), s32[]{:S(2)}) async-start(), calls=%async_computation | async-start | bytes 5242880 | tf_op jit(solution)/shard_map/all_gather | solution.py:18
  8.8 219.0 %all-gather.14.cloned.1.call-start = ((), (), s32[]{:S(2)}) async-start(), calls=%async_computation.4 | async-start | bytes 5242880 | tf_op jit(solution)/shard_map/all_gather | solution.py:36
  9.3 231.9 %all-gather.12.cloned.1.call-start = ((), (), s32[]{:S(2)}) async-start(), calls=%async_computation.3 | async-start | bytes 4718592 | tf_op jit(solution)/shard_map/all_gather | solution.py:33
Sparse Core Ops, SparseCore 0:
  9.2 55.2 all-gather.7
  66.3 52.5 all-gather.9
  120.8 52.5 all-gather.5
  175.1 52.5 all-gather.13
  229.1 12.1 all-gather.11
where the time goes:
time: 256 us; the launch traced here: 255 us
  waiting for transfers between devices  209 us (82%)
  matrix products  31.3 us (12%)
  between operations  13.2 us (5%)
    all_gather x1, waiting for transfers between devices, local(): inner = add_piece(lax.all_gather(inner_weight, 'fs', axis=0, tiled=True))  53.5 us
    all_gather x1, waiting for transfers between devices, local(): value = add_piece(lax.all_gather(value_weight, 'fs', axis=0, tiled=True))  47.6 us
    all_gather x1, waiting for transfers between devices, local(): outer = add_piece(lax.all_gather(outer_weight, 'fs', axis=0, tiled=True))  47.1 us
    all_gather x1, waiting for transfers between devices, local(): lax.all_gather(out_weight, 'fs', axis=0, tiled=True)  44.9 us
    dot_general x3, matrix products, add_piece(): return jnp.dot(normed, piece, preferred_element_type=jnp.float32)  23.6 us
    all_gather x1, waiting for transfers between devices, local(): everything = lax.all_gather(gated, 'tp', axis=1, tiled=True)  13.5 us
    dot_general x1, matrix products, local(): jnp.dot(everything, lax.all_gather(out_weight, 'fs', axis=0, tiled=True),...  7.7 us
  transfers between devices with their start and end apart: 5, of which 5 were waited for; matrix products, arithmetic and copies ran while one was open for 10% of the time, Pallas kernels for 0%

commit v1 on v0

v1 whole, which is shorter than its diff:
```python
import functools

import jax
import jax.numpy as jnp
from jax import lax
from jax.experimental import pallas as pl
from jax.experimental.pallas import tpu as pltpu
from jax.sharding import PartitionSpec as P

MESH = pl.DeviceIdType.MESH
F32 = jnp.float32
BF16 = jnp.bfloat16


def plain(tokens, norm_gain, outer_weight, inner_weight, value_weight, conv_taps, out_weight):
    batch, seq_len, width = tokens.shape
    xf = tokens.astype(F32)
    scale = lax.rsqrt(jnp.mean(xf * xf, axis=-1, keepdims=True) + 1e-06)
    normed = (xf * scale * norm_gain).astype(BF16).reshape(batch * seq_len, width)
    columns = outer_weight.shape[1]

    def project(weight):
        full = lax.all_gather(weight, "fs", axis=0, tiled=True)
        return jnp.dot(normed, full, preferred_element_type=F32).astype(BF16).astype(F32)

    outer, inner, value = project(outer_weight), project(inner_weight), project(value_weight)
    product = (inner * value).reshape(batch, seq_len, columns)
    offset = lax.axis_index("tp") * columns
    taps = lax.dynamic_slice_in_dim(conv_taps, offset, columns, 1)
    count = conv_taps.shape[0]
    padded = jnp.pad(product, ((0, 0), (count - 1, 0), (0, 0)))
    convolved = jnp.zeros((batch, seq_len, columns), F32)
    for k in range(count):
        convolved = convolved + taps[k] * padded[:, k : k + seq_len, :]
    gated = (outer * convolved.reshape(batch * seq_len, columns)).astype(BF16)
    everything = lax.all_gather(gated, "tp", axis=1, tiled=True)
    full = lax.all_gather(out_weight, "fs", axis=0, tiled=True)
    result = jnp.dot(everything, full, preferred_element_type=F32)
    return result.astype(BF16).reshape(batch, seq_len, columns)


def kernel(
    tok_hbm, gain_ref, outer_hbm, inner_hbm, value_hbm, taps_ref, outw_hbm, out_ref,
    tok, nm, wts, outw, acc, prod, gat, mine, osum, send_sems, recv_sems, local_sems,
):
    rep, fs, tp = lax.axis_index("rep"), lax.axis_index("fs"), lax.axis_index("tp")
    seq, width = tok_hbm.shape
    rows, cols = outer_hbm.shape
    half = cols // 2
    hrows = rows // 2
    count = taps_ref.shape[0]
    par = lax.rem(rep, 2)
    fx = fs + 1 - 2 * lax.rem(fs, 2)
    fy = lax.rem(fs + 2, 4)
    fd = 3 - fs
    shard = (fs, fx, fy, fd)
    to_x, to_y = (rep, fx, tp), (rep, fy, tp)
    to_z, to_t = (rep + 1 - 2 * par, fs, tp), (rep, fs, 1 - tp)
    used = [0]

    def remote(src, dst, device):
        k = used[0]
        used[0] += 1
        return pltpu.make_async_remote_copy(
            src_ref=src, dst_ref=dst, send_sem=send_sems.at[k], recv_sem=recv_sems.at[k],
            device_id=device, device_id_type=MESH,
        )

    barrier = pltpu.get_barrier_semaphore()
    for peer in (to_x, to_y, to_z, to_t):
        pl.semaphore_signal(barrier, inc=1, device_id=peer, device_id_type=MESH)

    hbm = (inner_hbm, value_hbm, outer_hbm)
    mycols = pl.ds(pl.multiple_of(par * half, half), half)
    loads = [pltpu.make_async_copy(tok_hbm, tok.at[0], local_sems.at[0])]
    for w in range(3):
        loads.append(pltpu.make_async_copy(hbm[w].at[:, mycols], wts.at[w, 0], local_sems.at[1 + w]))
    loads.append(pltpu.make_async_copy(outw_hbm, outw.at[0], local_sems.at[4]))
    for c in loads:
        c.start()

    chunks = 2
    crow = seq // 2 // chunks
    trow = [pl.ds(pl.multiple_of(tp * (seq // 2) + c * crow, 8), crow) for c in range(chunks)]
    tok_z = [remote(tok_hbm.at[r], tok.at[1, r], to_z) for r in trow]
    tok_t = [remote(tok.at[1, r], tok.at[1, r], to_t) for r in trow]
    w_x = [remote(hbm[w].at[:, mycols], wts.at[w, 1], to_x) for w in range(3)]
    w_y = [remote(hbm[w].at[:, mycols], wts.at[w, 2], to_y) for w in range(3)]
    low, high = pl.ds(0, hrows), pl.ds(hrows, hrows)
    d_x = [remote(wts.at[w, 2, low], wts.at[w, 3, low], to_x) for w in range(3)]
    d_y = [remote(wts.at[w, 1, high], wts.at[w, 3, high], to_y) for w in range(3)]
    o_x = [remote(outw_hbm.at[r], outw.at[1, r], to_x) for r in (high, low)]
    o_y = [remote(outw_hbm.at[r], outw.at[2, r], to_y) for r in (low, high)]
    od_x = remote(outw.at[2, low], outw.at[3, low], to_x)
    od_y = remote(outw.at[1, high], outw.at[3, high], to_y)
    group = tp * 2 + par
    other = tp * 2 + 1 - par
    g_z = remote(mine, gat.at[group], to_z)
    g_t = remote(gat.at[group], gat.at[group], to_t)
    g_f = remote(gat.at[other], gat.at[other], to_t)

    pl.semaphore_wait(barrier, 4)
    for w in range(3):
        w_x[w].start()
        w_y[w].start()
        if w < chunks:
            tok_z[w].start()

    tile = 128

    def norm(s):
        @pl.loop(0, seq // tile)
        def _(b):
            r = pl.multiple_of(b * tile, tile)
            xf = tok[s, pl.ds(r, tile), :].astype(F32)
            scale = lax.rsqrt(jnp.mean(xf * xf, axis=-1, keepdims=True) + 1e-06)
            y = (xf * scale * gain_ref[...]).astype(BF16)
            for j in range(4):
                nm[j, pl.ds(s * seq + r, tile), :] = y[:, j * rows : (j + 1) * rows]

    mt = 256

    def project(w, slots, start, length, fresh):
        @pl.loop(0, length // mt)
        def _(b):
            r = pl.ds(pl.multiple_of(start + b * mt, mt), mt)
            total = None
            for s in slots:
                d = jnp.dot(nm[shard[s], r, :], wts[w, s], preferred_element_type=F32)
                total = d if total is None else total + d
            if fresh:
                acc[w, r, :] = total
            else:
                acc[w, r, :] += total

    loads[0].wait()
    norm(0)
    for w in range(3):
        loads[1 + w].wait()
    loads[4].wait()
    for w in range(3):
        project(w, (0,), 0, seq, True)
    for w in range(3):
        w_y[w].wait_recv()
        d_x[w].start()
        w_x[w].wait_recv()
        d_y[w].start()
        if w == 2:
            for h in range(2):
                o_x[h].start()
                o_y[h].start()
        if w >= 1:
            tok_z[w - 1].wait_recv()
            tok_t[w - 1].start()
        project(w, (1, 2), 0, seq, False)
    tok_t[0].wait_recv()
    tok_t[1].wait_recv()
    norm(1)
    for w in range(3):
        project(w, (0, 1, 2), seq, seq, True)
    for w in range(3):
        d_x[w].wait_recv()
        d_y[w].wait_recv()
        project(w, (3,), 0, 2 * seq, False)

    tcols = pl.ds(pl.multiple_of(tp * cols + par * half, half), half)
    prod[0:8, :] = jnp.zeros((8, half), F32)

    def gate(s, store):
        @pl.loop(0, seq // tile)
        def _(b):
            r = pl.multiple_of(b * tile, tile)
            a = pl.ds(s * seq + r, tile)
            inner = acc[0, a, :].astype(BF16).astype(F32)
            value = acc[1, a, :].astype(BF16).astype(F32)
            outer = acc[2, a, :].astype(BF16).astype(F32)
            prod[pl.ds(r + 8, tile), :] = inner * value
            window = prod[pl.ds(r, tile + 8), :]
            conv = jnp.zeros((tile, half), F32)
            for k in range(count):
                lo = 8 - (count - 1) + k
                conv = conv + taps_ref[k : k + 1, tcols] * window[lo : lo + tile, :]
            store(pl.ds(r, tile), (outer * conv).astype(BF16))

    def keep_partner(r, x):
        mine[r, :] = x

    def keep_own(r, x):
        gat[group, r, :] = x

    gate(1, keep_partner)
    gate(0, keep_own)
    g_z.start()
    o_y[0].wait_recv()
    od_x.start()
    o_x[0].wait_recv()
    od_y.start()
    g_t.start()
    g_z.wait_recv()
    g_f.start()
    o_y[1].wait_recv()
    o_x[1].wait_recv()
    g_t.wait_recv()
    g_f.wait_recv()

    @pl.loop(0, seq // mt)
    def _(b):
        r = pl.ds(pl.multiple_of(b * mt, mt), mt)
        total = None
        for s in range(3):
            d = jnp.dot(gat[shard[s], r, :], outw[s], preferred_element_type=F32)
            total = d if total is None else total + d
        osum[r, :] = total

    od_x.wait_recv()
    od_y.wait_recv()

    @pl.loop(0, seq // mt)
    def _(b):
        r = pl.ds(pl.multiple_of(b * mt, mt), mt)
        d = jnp.dot(gat[fd, r, :], outw[3], preferred_element_type=F32)
        out_ref[r, :] = (osum[r, :] + d).astype(BF16)

    for c in tok_z + tok_t + w_x + w_y + d_x + d_y + o_x + o_y + [od_x, od_y, g_z, g_t, g_f]:
        c.wait_send()


COPIES = 25


def paired(tokens, norm_gain, outer_weight, inner_weight, value_weight, conv_taps, out_weight):
    _, seq, width = tokens.shape
    rows, cols = outer_weight.shape
    half = cols // 2
    anyspace = pl.BlockSpec(memory_space=pl.ANY)
    vmem = pl.BlockSpec(memory_space=pltpu.VMEM)
    out = pl.pallas_call(
        kernel,
        out_shape=jax.ShapeDtypeStruct((seq, cols), BF16),
        in_specs=[anyspace, vmem, anyspace, anyspace, anyspace, vmem, anyspace],
        out_specs=vmem,
        scratch_shapes=[
            pltpu.VMEM((2, seq, width), BF16),
            pltpu.VMEM((4, 2 * seq, rows), BF16),
            pltpu.VMEM((3, 4, rows, half), BF16),
            pltpu.VMEM((4, rows, cols), BF16),
            pltpu.VMEM((3, 2 * seq, half), F32),
            pltpu.VMEM((seq + 8, half), F32),
            pltpu.VMEM((4, seq, half), BF16),
            pltpu.VMEM((seq, half), BF16),
            pltpu.VMEM((seq, cols), F32),
            pltpu.SemaphoreType.DMA((COPIES,)),
            pltpu.SemaphoreType.DMA((COPIES,)),
            pltpu.SemaphoreType.DMA((5,)),
        ],
        compiler_params=pltpu.CompilerParams(
            collective_id=0, has_side_effects=True, vmem_limit_bytes=60 * 1024 * 1024
        ),
        name="mixer",
    )(
        tokens.reshape(seq, width), norm_gain.reshape(1, width), outer_weight, inner_weight,
        value_weight, conv_taps, out_weight,
    )
    return out.reshape(1, seq, cols)


def solution(mesh):
    shape = dict(mesh.shape)

    def local(tokens, *rest):
        rows, cols = rest[1].shape
        fits = (
            shape["fs"] == 4 and shape["tp"] == 2 and shape["rep"] % 2 == 0
            and tokens.shape[0] == 1 and tokens.shape[1] % 256 == 0
            and rows % 256 == 0 and cols == 2 * rows and rest[4].shape[0] <= 9
        )
        return (paired if fits else plain)(tokens, *rest)

    in_specs = (
        P(("rep", "fs"), None, None),
        P(),
        P("fs", "tp"),
        P("fs", "tp"),
        P("fs", "tp"),
        P(),
        P("fs", "tp"),
    )
    out_specs = P(("rep", "fs"), None, "tp")
    return jax.shard_map(local, mesh=mesh, in_specs=in_specs, out_specs=out_specs, check_vma=False)
```

time: 256 us -> 96.2 us (0.38)
  waiting for transfers between devices: 209 us -> 0 us
  Pallas kernels: 0 us -> 93.3 us
  matrix products: 31.3 us -> 0 us
  between operations: 13.2 us -> 0.01 us
    all_gather x5 -> x0, waiting for transfers between devices: 207 us -> none  [the longest x1 53.5 us: local(): inner = add_piece(lax.all_gather(inner_weight, 'fs', axis=0, tiled=True))]
    pallas_call x0 -> x1, Pallas kernels: none -> 93.3 us  [paired(): pl.pallas_call(kernel, out_shape=jax.ShapeDtypeStruct((seq, cols), BF16),...]
    dot_general x4 -> x0, matrix products: 31.3 us -> none  [the longest x3 23.6 us: add_piece(): return jnp.dot(normed, piece, preferred_element_type=jnp.float32)]
    unnamed x4 -> x1, local copies, waits for them, and re-layouts: 0.01 us -> 2.67 us
    unnamed x5 -> x0, waiting for transfers between devices: 2.63 us -> none
  transfers between devices with their start and end apart: 5 -> 0, of which waited for: 5 -> 0; matrix products, arithmetic and copies ran while one was open for 10% -> 0% of each run, Pallas kernels for 0% -> 0%
where the time goes in v1:
time: 96.2 us; the launch traced here: 95.9 us
  Pallas kernels  93.3 us (97%)
  local copies, waits for them, and re-layouts  2.67 us (3%)
    pallas_call x1, Pallas kernels, paired(): pl.pallas_call(kernel, out_shape=jax.ShapeDtypeStruct((seq, cols), BF16),...  93.3 us
    unnamed x1, local copies, waits for them, and re-layouts  2.67 us

profile of v1, /device:TPU:0, one launch (start us, length us, event | category | flops | bytes accessed | tf_op | source)
XLA Modules:
  0.0 95.9 jit_solution(5003634739478796270)
XLA Ops:
  0.0 93.3 %mixer.1 = bf16[768,1024]{1,0:T(8,128)(2,1)} custom-call(bf16[768,2048]{1,0:T(8,128)(2,1)} %bitcast.4, f32[1,2048]{1,0:T(1,128)} %bitcast.5, bf16[512,1024]{1,0:T(8,128)(2,1)} %outer_hbm.1, bf16[512,1024]{1,0:T(8,128)(2,1)} %inner_hbm.1, bf16[512,1024]{1,0:T(8,128)(2,1)} %value_hbm.1, f32[3,2048]{1,0:T(4,128)} %taps_ref.1, bf16[512,1024]{1,0:T(8,128)(2,1)} %outw_hbm.1), custom_call_target="tpu_custom_call" | custom-call | tf_op jit(solution)/shard_map/mixer/pallas_call | solution.py:237
  93.3 2.7 %copy.9 = bf16[1,768,1024]{2,1,0:T(8,128)(2,1)} copy(bf16[1,768,1024]{2,1,0:T(8,128)(2,1)} %bitcast.3) | data formatting | bytes 3145728

commit v2 on v1

v2 whole, which is shorter than its diff:
```python
import functools

import jax
import jax.numpy as jnp
from jax import lax
from jax.experimental import pallas as pl
from jax.experimental.pallas import tpu as pltpu
from jax.sharding import PartitionSpec as P

MESH = pl.DeviceIdType.MESH
F32 = jnp.float32
BF16 = jnp.bfloat16


def plain(tokens, norm_gain, outer_weight, inner_weight, value_weight, conv_taps, out_weight):
    batch, seq_len, width = tokens.shape
    xf = tokens.astype(F32)
    scale = lax.rsqrt(jnp.mean(xf * xf, axis=-1, keepdims=True) + 1e-06)
    normed = (xf * scale * norm_gain).astype(BF16).reshape(batch * seq_len, width)
    columns = outer_weight.shape[1]

    def project(weight):
        full = lax.all_gather(weight, "fs", axis=0, tiled=True)
        return jnp.dot(normed, full, preferred_element_type=F32).astype(BF16).astype(F32)

    outer, inner, value = project(outer_weight), project(inner_weight), project(value_weight)
    product = (inner * value).reshape(batch, seq_len, columns)
    offset = lax.axis_index("tp") * columns
    taps = lax.dynamic_slice_in_dim(conv_taps, offset, columns, 1)
    count = conv_taps.shape[0]
    padded = jnp.pad(product, ((0, 0), (count - 1, 0), (0, 0)))
    convolved = jnp.zeros((batch, seq_len, columns), F32)
    for k in range(count):
        convolved = convolved + taps[k] * padded[:, k : k + seq_len, :]
    gated = (outer * convolved.reshape(batch * seq_len, columns)).astype(BF16)
    everything = lax.all_gather(gated, "tp", axis=1, tiled=True)
    full = lax.all_gather(out_weight, "fs", axis=0, tiled=True)
    result = jnp.dot(everything, full, preferred_element_type=F32)
    return result.astype(BF16).reshape(batch, seq_len, columns)


def kernel(
    tok_hbm, gain_ref, outer_hbm, inner_hbm, value_hbm, taps_ref, outw_hbm, out_ref,
    tok, nm, wts, outw, acc, prod, gat, mine, osum, send_sems, recv_sems, local_sems,
):
    rep, fs, tp = lax.axis_index("rep"), lax.axis_index("fs"), lax.axis_index("tp")
    seq, width = tok_hbm.shape
    rows, cols = outer_hbm.shape
    half = cols // 2
    part = half // PARTS
    hrows = rows // 2
    count = taps_ref.shape[0]
    par = lax.rem(rep, 2)
    fx = fs + 1 - 2 * lax.rem(fs, 2)
    fy = lax.rem(fs + 2, 4)
    fd = 3 - fs
    shard = (fs, fx, fy, fd)
    to_x, to_y = (rep, fx, tp), (rep, fy, tp)
    to_z, to_t = (rep + 1 - 2 * par, fs, tp), (rep, fs, 1 - tp)
    used = [0]

    def remote(src, dst, device):
        k = used[0]
        used[0] += 1
        return pltpu.make_async_remote_copy(
            src_ref=src, dst_ref=dst, send_sem=send_sems.at[k], recv_sem=recv_sems.at[k],
            device_id=device, device_id_type=MESH,
        )

    barrier = pltpu.get_barrier_semaphore()
    for peer in (to_x, to_y, to_z, to_t):
        pl.semaphore_signal(barrier, inc=1, device_id=peer, device_id_type=MESH)

    hbm = (inner_hbm, value_hbm, outer_hbm)
    pieces = [(c, w) for c in range(PARTS) for w in range(3)]

    def mycols(c):
        return pl.ds(pl.multiple_of(par * half + c * part, part), part)

    tok_load = pltpu.make_async_copy(tok_hbm, tok.at[0], local_sems.at[0])
    ow_load = pltpu.make_async_copy(outw_hbm, outw.at[0], local_sems.at[1])
    w_load = {
        (c, w): pltpu.make_async_copy(hbm[w].at[:, mycols(c)], wts.at[c, w, 0], local_sems.at[2 + i])
        for i, (c, w) in enumerate(pieces)
    }
    tok_load.start()
    for p in pieces:
        w_load[p].start()
    ow_load.start()

    chunks = 2
    crow = seq // 2 // chunks
    trow = [pl.ds(pl.multiple_of(tp * (seq // 2) + c * crow, 8), crow) for c in range(chunks)]
    tok_z = [remote(tok_hbm.at[r], tok.at[1, r], to_z) for r in trow]
    tok_t = [remote(tok.at[1, r], tok.at[1, r], to_t) for r in trow]
    low, high = pl.ds(0, hrows), pl.ds(hrows, hrows)
    w_x, w_y, d_x, d_y = {}, {}, {}, {}
    for c, w in pieces:
        src = hbm[w].at[:, mycols(c)]
        w_x[c, w] = remote(src, wts.at[c, w, 1], to_x)
        w_y[c, w] = remote(src, wts.at[c, w, 2], to_y)
        d_x[c, w] = remote(wts.at[c, w, 2, low], wts.at[c, w, 3, low], to_x)
        d_y[c, w] = remote(wts.at[c, w, 1, high], wts.at[c, w, 3, high], to_y)
    one = pl.ds(pl.multiple_of(par * hrows, hrows), hrows)
    two = pl.ds(pl.multiple_of((1 - par) * hrows, hrows), hrows)
    o_y = remote(outw_hbm.at[one], outw.at[2, one], to_y)
    o_x = remote(outw_hbm.at[two], outw.at[1, two], to_x)
    oz_y = remote(outw.at[2, one], outw.at[2, one], to_z)
    oz_x = remote(outw.at[1, two], outw.at[1, two], to_z)
    od_x = remote(outw.at[2, one], outw.at[3, one], to_x)
    od_y = remote(outw.at[1, two], outw.at[3, two], to_y)
    group, other = tp * 2 + par, tp * 2 + 1 - par
    peer_group, peer_other = (1 - tp) * 2 + par, (1 - tp) * 2 + 1 - par
    g_z = [remote(mine.at[c], gat.at[group, c], to_z) for c in range(PARTS)]
    g_t = [remote(gat.at[group, c], gat.at[group, c], to_t) for c in range(PARTS)]
    g_f = [remote(gat.at[other, c], gat.at[other, c], to_t) for c in range(PARTS)]

    pl.semaphore_wait(barrier, 4)
    for r in range(chunks):
        tok_z[r].start()
    for w in range(3):
        w_x[0, w].start()
        w_y[0, w].start()

    tile = 128

    def norm(s):
        @pl.loop(0, seq // tile)
        def _(b):
            r = pl.multiple_of(b * tile, tile)
            xf = tok[s, pl.ds(r, tile), :].astype(F32)
            scale = lax.rsqrt(jnp.mean(xf * xf, axis=-1, keepdims=True) + 1e-06)
            y = (xf * scale * gain_ref[...]).astype(BF16)
            for j in range(4):
                nm[j, pl.ds(s * seq + r, tile), :] = y[:, j * rows : (j + 1) * rows]

    mt = 256

    def project(c, w, slots, start, length, fresh):
        @pl.loop(0, length // mt)
        def _(b):
            r = pl.ds(pl.multiple_of(start + b * mt, mt), mt)
            total = None
            for s in slots:
                d = jnp.dot(nm[shard[s], r, :], wts[c, w, s], preferred_element_type=F32)
                total = d if total is None else total + d
            if fresh:
                acc[c, w, r, :] = total
            else:
                acc[c, w, r, :] += total

    prod[0:8, :] = jnp.zeros((8, part), F32)

    def gate(c, s, store):
        tcols = pl.ds(pl.multiple_of(tp * cols + par * half + c * part, part), part)

        @pl.loop(0, seq // tile)
        def _(b):
            r = pl.multiple_of(b * tile, tile)
            a = pl.ds(s * seq + r, tile)
            inner = acc[c, 0, a, :].astype(BF16).astype(F32)
            value = acc[c, 1, a, :].astype(BF16).astype(F32)
            outer = acc[c, 2, a, :].astype(BF16).astype(F32)
            prod[pl.ds(r + 8, tile), :] = inner * value
            window = prod[pl.ds(r, tile + 8), :]
            conv = jnp.zeros((tile, part), F32)
            for k in range(count):
                lo = 8 - (count - 1) + k
                conv = conv + taps_ref[k : k + 1, tcols] * window[lo : lo + tile, :]
            store(pl.ds(r, tile), (outer * conv).astype(BF16))

    def keep_partner(c):
        def store(r, x):
            mine[c, r, :] = x
        return store

    def keep_own(c):
        def store(r, x):
            gat[group, c, r, :] = x
        return store

    tok_load.wait()
    norm(0)
    for w in range(3):
        w_load[0, w].wait()
        w_y[0, w].wait_recv()
        d_x[0, w].start()
        w_x[0, w].wait_recv()
        d_y[0, w].start()
        if w == 2:
            o_y.start()
            o_x.start()
            for v in range(3):
                w_x[1, v].start()
                w_y[1, v].start()
        project(0, w, (0, 1, 2), 0, seq, True)
    tok_z[0].wait_recv()
    tok_t[0].start()
    for w in range(3):
        d_x[0, w].wait_recv()
        d_y[0, w].wait_recv()
        project(0, w, (3,), 0, seq, False)
    for w in range(3):
        w_load[1, w].wait()
        project(1, w, (0,), 0, seq, True)
    tok_z[1].wait_recv()
    tok_t[1].start()
    o_y.wait_recv()
    oz_y.start()
    o_x.wait_recv()
    oz_x.start()
    gate(0, 0, keep_own(0))
    tok_t[0].wait_recv()
    tok_t[1].wait_recv()
    norm(1)
    g_t[0].start()
    for w in range(3):
        project(0, w, (0, 1, 2, 3), seq, seq, True)
    w_y[1, 0].wait_recv()
    d_x[1, 0].start()
    w_x[1, 0].wait_recv()
    d_y[1, 0].start()
    gate(0, 1, keep_partner(0))
    for w in range(3):
        if w > 0:
            w_y[1, w].wait_recv()
            d_x[1, w].start()
            w_x[1, w].wait_recv()
            d_y[1, w].start()
        else:
            project(1, w, (1, 2), 0, seq, False)
            g_z[0].start()
        if w == 2:
            od_x.start()
            od_y.start()
        if w > 0:
            project(1, w, (1, 2), 0, seq, False)
        project(1, w, (0, 1, 2), seq, seq, True)
    for w in range(3):
        d_x[1, w].wait_recv()
        d_y[1, w].wait_recv()
        project(1, w, (3,), seq, seq, False)
        if w < 2:
            project(1, w, (3,), 0, seq, False)
    gate(1, 1, keep_partner(1))
    project(1, 2, (3,), 0, seq, False)
    g_z[1].start()
    gate(1, 0, keep_own(1))
    g_z[0].wait_recv()
    g_f[0].start()
    g_t[0].wait_recv()
    oz_y.wait_recv()
    oz_x.wait_recv()
    ow_load.wait()
    g_t[1].start()
    g_f[0].wait_recv()

    def slot(g):
        return lax.rem(g + fs, 2) + 2 * lax.rem(g // 2 + fs // 2, 2)

    def mix(terms, first, last):
        @pl.loop(0, seq // mt)
        def _(b):
            r = pl.ds(pl.multiple_of(b * mt, mt), mt)
            total = None
            for g, s, c in terms:
                d = jnp.dot(
                    gat[g, c, r, :], outw[s, c * part : (c + 1) * part, :],
                    preferred_element_type=F32,
                )
                total = d if total is None else total + d
            if not first:
                total = total + osum[r, :]
            if last:
                out_ref[r, :] = total.astype(BF16)
            else:
                osum[r, :] = total

    mix([(shard[s], s, 0) for s in range(3)], True, False)
    od_x.wait_recv()
    od_y.wait_recv()
    g_t[1].wait_recv()
    mix([(fd, 3, 0), (group, slot(group), 1), (peer_group, slot(peer_group), 1)], False, False)
    g_z[1].wait_recv()
    g_f[1].start()
    g_f[1].wait_recv()
    mix([(other, slot(other), 1), (peer_other, slot(peer_other), 1)], False, True)

    sent = tok_z + tok_t + [o_x, o_y, oz_x, oz_y, od_x, od_y] + g_z + g_t + g_f
    for p in pieces:
        sent += [w_x[p], w_y[p], d_x[p], d_y[p]]
    for c in sent:
        c.wait_send()


PARTS = 2
COPIES = 40


def paired(tokens, norm_gain, outer_weight, inner_weight, value_weight, conv_taps, out_weight):
    _, seq, width = tokens.shape
    rows, cols = outer_weight.shape
    half = cols // 2
    anyspace = pl.BlockSpec(memory_space=pl.ANY)
    vmem = pl.BlockSpec(memory_space=pltpu.VMEM)
    out = pl.pallas_call(
        kernel,
        out_shape=jax.ShapeDtypeStruct((seq, cols), BF16),
        in_specs=[anyspace, vmem, anyspace, anyspace, anyspace, vmem, anyspace],
        out_specs=vmem,
        scratch_shapes=[
            pltpu.VMEM((2, seq, width), BF16),
            pltpu.VMEM((4, 2 * seq, rows), BF16),
            pltpu.VMEM((PARTS, 3, 4, rows, half // PARTS), BF16),
            pltpu.VMEM((4, rows, cols), BF16),
            pltpu.VMEM((PARTS, 3, 2 * seq, half // PARTS), F32),
            pltpu.VMEM((seq + 8, half // PARTS), F32),
            pltpu.VMEM((4, PARTS, seq, half // PARTS), BF16),
            pltpu.VMEM((PARTS, seq, half // PARTS), BF16),
            pltpu.VMEM((seq, cols), F32),
            pltpu.SemaphoreType.DMA((COPIES,)),
            pltpu.SemaphoreType.DMA((COPIES,)),
            pltpu.SemaphoreType.DMA((2 + 3 * PARTS,)),
        ],
        compiler_params=pltpu.CompilerParams(
            collective_id=0, has_side_effects=True, vmem_limit_bytes=60 * 1024 * 1024
        ),
        name="mixer",
    )(
        tokens.reshape(seq, width), norm_gain.reshape(1, width), outer_weight, inner_weight,
        value_weight, conv_taps, out_weight,
    )
    return out.reshape(1, seq, cols)


def solution(mesh):
    shape = dict(mesh.shape)

    def local(tokens, *rest):
        rows, cols = rest[1].shape
        fits = (
            shape["fs"] == 4 and shape["tp"] == 2 and shape["rep"] % 2 == 0
            and tokens.shape[0] == 1 and tokens.shape[1] % 256 == 0
            and rows % 256 == 0 and cols == 2 * rows and rest[4].shape[0] <= 9
        )
        return (paired if fits else plain)(tokens, *rest)

    in_specs = (
        P(("rep", "fs"), None, None),
        P(),
        P("fs", "tp"),
        P("fs", "tp"),
        P("fs", "tp"),
        P(),
        P("fs", "tp"),
    )
    out_specs = P(("rep", "fs"), None, "tp")
    return jax.shard_map(local, mesh=mesh, in_specs=in_specs, out_specs=out_specs, check_vma=False)
```

time: 96.2 us -> 90.6 us (0.942)
  Pallas kernels: 93.3 us -> 87.4 us
    pallas_call x1, Pallas kernels: 93.3 us -> 87.4 us  [paired(): pl.pallas_call(kernel, out_shape=jax.ShapeDtypeStruct((seq, cols), BF16),...]
where the time goes in v2:
time: 90.6 us; the launch traced here: 90.1 us
  Pallas kernels  87.4 us (96%)
  local copies, waits for them, and re-layouts  2.67 us (3%)
    pallas_call x1, Pallas kernels, paired(): pl.pallas_call(kernel, out_shape=jax.ShapeDtypeStruct((seq, cols), BF16),...  87.4 us
    unnamed x1, local copies, waits for them, and re-layouts  2.67 us

profile of v2, /device:TPU:0, one launch (start us, length us, event | category | flops | bytes accessed | tf_op | source)
XLA Modules:
  0.0 90.1 jit_solution(1646720752746209727)
XLA Ops:
  0.0 87.4 %mixer.1 = bf16[768,1024]{1,0:T(8,128)(2,1)} custom-call(bf16[768,2048]{1,0:T(8,128)(2,1)} %bitcast.4, f32[1,2048]{1,0:T(1,128)} %bitcast.5, bf16[512,1024]{1,0:T(8,128)(2,1)} %outer_hbm.1, bf16[512,1024]{1,0:T(8,128)(2,1)} %inner_hbm.1, bf16[512,1024]{1,0:T(8,128)(2,1)} %value_hbm.1, f32[3,2048]{1,0:T(4,128)} %taps_ref.1, bf16[512,1024]{1,0:T(8,128)(2,1)} %outw_hbm.1), custom_call_target="tpu_custom_call" | custom-call | tf_op jit(solution)/shard_map/mixer/pallas_call | solution.py:306
  87.4 2.7 %copy.9 = bf16[1,768,1024]{2,1,0:T(8,128)(2,1)} copy(bf16[1,768,1024]{2,1,0:T(8,128)(2,1)} %bitcast.3) | data formatting | bytes 3145728

commit v3 on v2

--- a/solution.py
+++ b/solution.py
@@ -121,6 +121,8 @@
     for w in range(3):
         w_x[0, w].start()
         w_y[0, w].start()
+    o_y.start()
+    o_x.start()
 
     tile = 128
 
@@ -188,8 +190,6 @@
         w_x[0, w].wait_recv()
         d_y[0, w].start()
         if w == 2:
-            o_y.start()
-            o_x.start()
             for v in range(3):
                 w_x[1, v].start()
                 w_y[1, v].start()
@@ -197,18 +197,18 @@
     tok_z[0].wait_recv()
     tok_t[0].start()
     for w in range(3):
-        d_x[0, w].wait_recv()
-        d_y[0, w].wait_recv()
-        project(0, w, (3,), 0, seq, False)
-    for w in range(3):
         w_load[1, w].wait()
         project(1, w, (0,), 0, seq, True)
-    tok_z[1].wait_recv()
-    tok_t[1].start()
     o_y.wait_recv()
     oz_y.start()
     o_x.wait_recv()
     oz_x.start()
+    tok_z[1].wait_recv()
+    tok_t[1].start()
+    for w in range(3):
+        d_x[0, w].wait_recv()
+        d_y[0, w].wait_recv()
+        project(0, w, (3,), 0, seq, False)
     gate(0, 0, keep_own(0))
     tok_t[0].wait_recv()
     tok_t[1].wait_recv()
@@ -283,8 +283,9 @@
     mix([(fd, 3, 0), (group, slot(group), 1), (peer_group, slot(peer_group), 1)], False, False)
     g_z[1].wait_recv()
     g_f[1].start()
+    mix([(other, slot(other), 1)], False, False)
     g_f[1].wait_recv()
-    mix([(other, slot(other), 1), (peer_other, slot(peer_other), 1)], False, True)
+    mix([(peer_other, slot(peer_other), 1)], False, True)
 
     sent = tok_z + tok_t + [o_x, o_y, oz_x, oz_y, od_x, od_y] + g_z + g_t + g_f
     for p in pieces:
@@ -301,11 +302,11 @@
     _, seq, width = tokens.shape
     rows, cols = outer_weight.shape
     half = cols // 2
-    anyspace = pl.BlockSpec(memory_space=pl.ANY)
+    anyspace = pl.BlockSpec(memory_space=pltpu.HBM)
     vmem = pl.BlockSpec(memory_space=pltpu.VMEM)
     out = pl.pallas_call(
         kernel,
-        out_shape=jax.ShapeDtypeStruct((seq, cols), BF16),
+        out_shape=pltpu.VMEM((seq, cols), BF16),
         in_specs=[anyspace, vmem, anyspace, anyspace, anyspace, vmem, anyspace],
         out_specs=vmem,
         scratch_shapes=[
@@ -323,7 +324,7 @@
             pltpu.SemaphoreType.DMA((2 + 3 * PARTS,)),
         ],
         compiler_params=pltpu.CompilerParams(
-            collective_id=0, has_side_effects=True, vmem_limit_bytes=60 * 1024 * 1024
+            collective_id=0, has_side_effects=True, vmem_limit_bytes=58 * 1024 * 1024
         ),
         name="mixer",
     )(

time: 90.6 us -> 85.2 us (0.940)
  Pallas kernels: 87.4 us -> 83.5 us
  local copies, waits for them, and re-layouts: 2.67 us -> 1.15 us
    pallas_call x1, Pallas kernels: 87.4 us -> 83.5 us  [paired(): pl.pallas_call(kernel, out_shape=pltpu.VMEM((seq, cols), BF16), in_specs=...]
    unnamed x1, local copies, waits for them, and re-layouts: 2.67 us -> 1.15 us
where the time goes in v3:
time: 85.2 us; the launch traced here: 84.7 us
  Pallas kernels  83.5 us (98%)
  local copies, waits for them, and re-layouts  1.15 us (1%)
    pallas_call x1, Pallas kernels, paired(): pl.pallas_call(kernel, out_shape=pltpu.VMEM((seq, cols), BF16), in_specs=...  83.5 us

profile of v3, /device:TPU:0, one launch (start us, length us, event | category | flops | bytes accessed | tf_op | source)
XLA Modules:
  0.0 84.7 jit_solution(2563503430617781477)
XLA Ops:
  0.0 83.5 %mixer.1 = bf16[768,1024]{1,0:T(8,128)(2,1)S(1)} custom-call(bf16[768,2048]{1,0:T(8,128)(2,1)} %bitcast.4, f32[1,2048]{1,0:T(1,128)} %bitcast.5, bf16[512,1024]{1,0:T(8,128)(2,1)} %outer_hbm.1, bf16[512,1024]{1,0:T(8,128)(2,1)} %inner_hbm.1, bf16[512,1024]{1,0:T(8,128)(2,1)} %value_hbm.1, f32[3,2048]{1,0:T(4,128)} %taps_ref.1, bf16[512,1024]{1,0:T(8,128)(2,1)} %outw_hbm.1), custom_call_target="tpu_custom_call" | custom-call | tf_op jit(solution)/shard_map/mixer/pallas_call | solution.py:307
  83.5 1.1 %copy.9 = bf16[1,768,1024]{2,1,0:T(8,128)(2,1)} copy(bf16[1,768,1024]{2,1,0:T(8,128)(2,1)S(1)} %bitcast.3) | data formatting | bytes 3145728
